TPU v7x, 512 devices: a 8x2x16 block of a 8x8x16 slice. The times are simulated.
512 devices in a mesh: grp: 2 (over y), sp: 16 (over z), tp: 16 (over x, core).
Axes of the slice: x: 8, y: 2, z: 16, core: 2. Of those that a mesh axis runs over, the one named last changes fastest.
The devices are a block of a 8x8x16 slice.
Arguments:
- target: bfloat16 [4096, 2048], P(('grp', 'sp', 'tp')), parts along dimension 0, may hold values from -5 to 5
- source: bfloat16 [32768, 2048], P(('grp', 'sp', 'tp')), parts along dimension 0, may hold values from -5 to 5
- source_gain: float32 [2048], replicated, may hold values from 0.1 to 1.9
- pre_first: float32 [2048], replicated, may hold values from 0.1 to 1.9
- query_first: bfloat16 [2048, 2048], P(None, 'tp')
- keyval_first: bfloat16 [2048, 1024], P(None, 'tp')
- out_first: bfloat16 [2048, 2048], P('tp'), may hold values from -0.125 to 0.125
- post_first: float32 [2048], replicated, may hold values from 0.1 to 1.9
- ffn_pre: float32 [2048], replicated, may hold values from 0.1 to 1.9
- w_gate: bfloat16 [2048, 2816], P(None, 'tp'), may hold values from -0.125 to 0.125
- w_value: bfloat16 [2048, 2816], P(None, 'tp'), may hold values from -0.125 to 0.125
- conv_gate: float32 [3, 2816], P(None, 'tp'), may hold values from -3.5 to 3.5
- conv_value: float32 [3, 2816], P(None, 'tp'), may hold values from -3.5 to 3.5
- w_down: bfloat16 [2816, 2048], P('tp'), may hold values from -0.109375 to 0.109375
- ffn_post: float32 [2048], replicated, may hold values from 0.1 to 1.9
- pre_second: float32 [2048], replicated, may hold values from 0.1 to 1.9
- query_second: bfloat16 [2048, 2048], P(None, 'tp')
- keyval_second: bfloat16 [2048, 1024], P(None, 'tp')
- out_second: bfloat16 [2048, 2048], P('tp'), may hold values from -0.125 to 0.125
- post_second: float32 [2048], replicated, may hold values from 0.1 to 1.9
Outputs:
- decoded: float32 [4096, 2048], P(('grp', 'sp', 'tp')), parts along dimension 0
There are 2 independent parts, one for each index of `grp`. A program takes and returns all parts, laid end to end along the dimension named above; an argument that names none is the same for every part. Nothing has to cross between parts.
All inputs are finite; a program needn't handle non-finite values.
Results may differ from a plain program's by a relative error of at most 0.04.
Values may be sent and summed in bfloat16 or wider, within the bound.
A program may use at most 128 MiB of HBM per device.

v0:
```python
import jax
import jax.numpy as jnp
from jax import lax
from jax.sharding import PartitionSpec as P

HEAD = 128
KVH = 4


def in_blocks(array, dim, size):
    before, after = (array.shape[:dim], array.shape[dim + 1 :])
    return jnp.moveaxis(array.reshape(*before, size, -1, *after), dim, 0)


def sent_and_summed(array, axis, dim):
    parts = in_blocks(array, dim, lax.axis_size(axis))
    arrived = lax.all_to_all(parts, axis, split_axis=0, concat_axis=0, tiled=True)
    return arrived.astype(jnp.float32).sum(axis=0)


def swapped(block, axis, distance):
    count = lax.axis_size(axis)
    route = []
    for low in range(count):
        high = low | 1 << distance
        if high != low and high < count:
            route += [(low, high), (high, low)]
    return lax.ppermute(block, axis, route)


def in_one_piece(arrays, axis, dim, along):
    both = jnp.concatenate(arrays, axis=along)
    result, at, done = (lax.all_gather(both, axis, axis=dim, tiled=True), 0, [])
    for a in arrays:
        done.append(lax.slice_in_dim(result, at, at + a.shape[along], axis=along))
        at += a.shape[along]
    return tuple(done)


def shifted(value, axis, steps):
    count = lax.axis_size(axis)
    leading, last = (max(0, -steps), min(count, count - steps))
    return lax.ppermute(value, axis, [(source, source + steps) for source in range(leading, last)])


def normed(values, gain):
    widened = values.astype(jnp.float32)
    return widened * lax.rsqrt(jnp.mean(widened * widened, axis=-1, keepdims=True) + 1e-06) * gain


def project_rows(rows_here, weights):
    shard_rows = lax.all_gather(rows_here, "tp", axis=0, tiled=True)
    products = [
        jnp.dot(shard_rows, weight, preferred_element_type=jnp.float32).astype(jnp.bfloat16)
        for weight in weights
    ]
    return jnp.concatenate(products, axis=1)


def summed_rows(parts, weight):
    return sent_and_summed(
        jnp.dot(parts, weight, preferred_element_type=jnp.float32).astype(jnp.bfloat16), "tp", 0
    )


def key_columns(source_rows, keyval_first, keyval_second):
    both_layers = jnp.concatenate([keyval_first, keyval_second], axis=1)
    columns = jnp.einsum(
        "rd,dc->cr",
        lax.all_gather(source_rows, "tp", axis=0, tiled=True),
        both_layers,
        preferred_element_type=jnp.float32,
    ).astype(jnp.bfloat16)
    column_count = keyval_first.shape[1]
    stacked = columns.reshape(2, column_count, columns.shape[1])
    own_index = lax.axis_index("tp")
    doublings = (2 * HEAD // column_count).bit_length() - 1
    for bit_number in range(doublings):
        lower_half = own_index // 2**bit_number % 2 == 0
        half_rows = stacked.shape[2] // 2
        outgoing = jnp.where(lower_half, stacked[:, :, half_rows:], stacked[:, :, :half_rows])
        retained = jnp.where(lower_half, stacked[:, :, :half_rows], stacked[:, :, half_rows:])
        partner = swapped(outgoing, "tp", bit_number)
        stacked = jnp.where(
            lower_half,
            jnp.concatenate([retained, partner], axis=1),
            jnp.concatenate([partner, retained], axis=1),
        )
    return (stacked[:, :HEAD], stacked[:, HEAD:])


def absorber(query_heads, running, shard_pair):
    scale_factor = HEAD ** (-0.5)
    best_score, weight_sum, weighted = running
    key_block, value_block = shard_pair
    scores = (
        jnp.einsum("thd,ds->ths", query_heads, key_block, preferred_element_type=jnp.float32)
        * scale_factor
    )
    newest = jnp.max(scores, axis=2)
    rescale = jnp.exp(best_score - newest)
    weights = jnp.exp(scores - newest[:, :, None])
    weight_sum = weight_sum * rescale + jnp.sum(weights, axis=2)
    weighted = weighted * rescale[:, :, None] + jnp.einsum(
        "ths,ds->thd", weights.astype(jnp.bfloat16), value_block, preferred_element_type=jnp.float32
    )
    return (newest, weight_sum, weighted)


def empty_running(row_count, head_count):
    return (
        jnp.full((row_count, head_count), -jnp.inf, jnp.float32),
        jnp.zeros((row_count, head_count), jnp.float32),
        jnp.zeros((row_count, head_count, HEAD), jnp.float32),
    )


def attend_shares(queries, keys_t, values_t):
    row_count = queries.shape[0]
    own_heads = queries.shape[1] // HEAD
    group_count = lax.axis_size("tp") // KVH
    doublings = group_count.bit_length() - 1
    own_index = lax.axis_index("tp")
    grouped = queries
    for bit_number in range(doublings):
        lower_half = own_index // 2**bit_number % 2 == 0
        partner = swapped(grouped, "tp", bit_number)
        grouped = jnp.where(
            lower_half,
            jnp.concatenate([grouped, partner], axis=1),
            jnp.concatenate([partner, grouped], axis=1),
        )
    head_count = grouped.shape[1] // HEAD
    query_heads = grouped.reshape(row_count, head_count, HEAD)
    best_score, weight_sum, weighted = absorber(
        query_heads,
        empty_running(row_count, head_count),
        in_one_piece((keys_t, values_t), "sp", 1, 0),
    )
    for bit_number in range(doublings):
        other_best, other_sum, other_weighted = (
            swapped(best_score.astype(jnp.bfloat16), "tp", bit_number).astype(best_score.dtype),
            swapped(weight_sum.astype(jnp.bfloat16), "tp", bit_number).astype(weight_sum.dtype),
            swapped(weighted.astype(jnp.bfloat16), "tp", bit_number).astype(weighted.dtype),
        )
        newest = jnp.maximum(best_score, other_best)
        own_scale = jnp.exp(best_score - newest)
        other_scale = jnp.exp(other_best - newest)
        weight_sum = weight_sum * own_scale + other_sum * other_scale
        weighted = weighted * own_scale[:, :, None] + other_weighted * other_scale[:, :, None]
        best_score = newest
    first_head = own_index % group_count * own_heads
    chosen = lax.dynamic_slice_in_dim(weighted, first_head, own_heads, 1)
    chosen_sums = lax.dynamic_slice_in_dim(weight_sum, first_head, own_heads, 1)
    return (
        (chosen / chosen_sums[:, :, None]).reshape(row_count, own_heads * HEAD).astype(jnp.bfloat16)
    )


def causal_mix(rim_rows, up_rows, conv_taps):
    padded = jnp.concatenate([rim_rows, up_rows], axis=0).astype(jnp.float32)
    length = up_rows.shape[0]
    return (
        conv_taps[0] * padded[:length]
        + conv_taps[1] * padded[1 : length + 1]
        + conv_taps[2] * padded[2:]
    )


def per_device(
    target,
    source,
    source_gain,
    pre_first,
    query_first,
    keyval_first,
    out_first,
    post_first,
    ffn_pre,
    w_gate,
    w_value,
    conv_gate,
    conv_value,
    w_down,
    ffn_post,
    pre_second,
    query_second,
    keyval_second,
    out_second,
    post_second,
):
    source_rows = normed(source, source_gain).astype(jnp.bfloat16)
    keys_t, values_t = key_columns(source_rows, keyval_first, keyval_second)

    def attention_layer(stream, pre_gain, w_query, layer_index, w_out, post_gain):
        queries = project_rows(normed(stream, pre_gain).astype(jnp.bfloat16), (w_query,))
        heads = attend_shares(queries, keys_t[layer_index], values_t[layer_index])
        mixed = summed_rows(heads, w_out)
        return stream.astype(jnp.float32) + normed(mixed, post_gain)

    after_first = attention_layer(target, pre_first, query_first, 0, out_first, post_first)
    up_both = project_rows(normed(after_first, ffn_pre).astype(jnp.bfloat16), (w_gate, w_value))
    hidden_width = w_gate.shape[1]
    up_gate = up_both[:, :hidden_width]
    up_value = up_both[:, hidden_width:]
    rim_gate, rim_value = shifted((up_gate[-2:], up_value[-2:]), "sp", 1)
    gated = (
        jax.nn.gelu(causal_mix(rim_gate, up_gate, conv_gate), approximate=True)
        * causal_mix(rim_value, up_value, conv_value)
    ).astype(jnp.bfloat16)
    ffn_sum = summed_rows(gated, w_down)
    after_ffn = after_first + normed(ffn_sum, ffn_post)
    return attention_layer(after_ffn, pre_second, query_second, 1, out_second, post_second)


def solution(mesh):
    placed = (
        P(("grp", "sp", "tp"), None),
        P(("grp", "sp", "tp"), None),
        P(),
        P(),
        P(None, "tp"),
        P(None, "tp"),
        P("tp", None),
        P(),
        P(),
        P(None, "tp"),
        P(None, "tp"),
        P(None, "tp"),
        P(None, "tp"),
        P("tp", None),
        P(),
        P(),
        P(None, "tp"),
        P(None, "tp"),
        P("tp", None),
        P(),
    )
    return jax.shard_map(
        per_device,
        mesh=mesh,
        in_specs=placed,
        out_specs=P(("grp", "sp", "tp"), None),
        check_vma=False,
    )
```

profile of v0, /device:TPU:65, one launch (start us, length us, event | category | flops | bytes accessed | tf_op | source)
XLA Modules:
  0.0 380.8 jit_solution(5917875736320434852)
XLA Ops:
  6.6 1.2 fusion.19
  7.8 1.8 fusion.21
  9.8 83.2 %all-gather.4.cloned.1.call-done = bf16[1024,2048]{1,0:T(8,128)(2,1)} async-done(((bf16[64,2048]{1,0:T(8,128)(2,1)}), bf16[1024,2048]{1,0:T(8,128)(2,1)}) %all-gather.4.cloned.1.call-update) | async-done | bytes 4194320 | tf_op jit(solution)/shard_map/all_gather | solution.py:70
  93.0 3.9 %convolution_convert_fusion.3 = bf16[128,1024]{1,0:T(8,128)(2,1)S(1)} fusion(bf16[1024,2048]{1,0:T(8,128)(2,1)} %all-gather.4.cloned.1.call-done, bf16[2048,64]{0,1:T(8,128)(2,1)} %param.37, bf16[2048,64]{0,1:T(8,128)(2,1)} %param.25), kind=kOutput, calls=%fused_computation.16 | convolution fusion | flops 538050560 | bytes 4980736 | tf_op jit(solution)/shard_map/rd,dc->cr/dot_general | solution.py:68
  96.9 2.2 collective-permute-start.2
  99.1 1.0 collective-permute-done.2
  100.2 3.0 collective-permute-start.3
  103.3 3.7 collective-permute-done.3
  107.0 0.7 slice_bitcast_fusion.9
  107.7 0.7 pad_maximum_fusion
  108.7 18.7 %all_gather.18 = bf16[128,2048]{1,0:T(8,128)(2,1)S(1)} all-gather(bf16[8,2048]{1,0:T(8,128)(2,1)S(1)} %fusion.52), channel_id=1, replica_groups=mesh['grp'=2,'sp'=16,'tp'=16] {'tp'}, dimensions={0}, use_global_device_ids=true | all-gather | bytes 557056 | tf_op jit(solution)/shard_map/all_gather | solution.py:52
  127.7 2.1 collective-permute-start
  129.8 1.0 collective-permute-done
  130.9 2.0 collective-permute-start.1
  132.8 3.5 collective-permute-done.1
  136.4 41.9 %all-gather.6.cloned.1.call-done = bf16[256,4096]{1,0:T(8,128)(2,1)} async-done(((bf16[256,256]{1,0:T(8,128)(2,1)}), bf16[256,4096]{1,0:T(8,128)(2,1)}) %all-gather.6.cloned.1.call-update) | async-done | bytes 2097168 | tf_op jit(solution)/shard_map/all_gather | solution.py:33
  178.3 2.7 multiply_reduce_fusion.1
  181.1 1.5 fusion
  182.7 13.7 %collective-permute-start.4 = (bf16[128,4]{0,1:T(4,128)(2,1)S(1)}, bf16[128,4]{0,1:T(4,128)(2,1)S(1)}, u32[]{:S(2)}, u32[]{:S(2)}) collective-permute-start(bf16[128,4]{0,1:T(4,128)(2,1)S(1)} %get-tuple-element.43), channel_id=1, source_target_pairs={{0,1},{1,0},{2,3},{3,2},{4,5},{5,4},{6,7},{7,6},{8,9},{9,8},{10,11... | collective-permute-start | bytes 3080 | tf_op jit(solution)/shard_map/ppermute | solution.py:28
  196.4 2.0 collective-permute-start.8
  198.4 3.5 collective-permute-start.6
  201.9 2.0 collective-permute-start.9
  203.9 2.4 collective-permute-done.9
  206.2 0.6 multiply_add_fusion.6
  206.8 2.3 fusion.109
  209.2 4.0 %collective-permute-start.5 = (bf16[128,4,128]{2,0,1:T(8,128)(2,1)}, bf16[128,4,128]{2,0,1:T(8,128)(2,1)}, u32[]{:S(2)}, u32[]{:S(2)}) collective-permute-start(bf16[128,4,128]{2,0,1:T(8,128)(2,1)} %get-tuple-element.47), channel_id=1, source_target_pairs={{0,1},{1,0},{2,3},{3,2},{4,5},{5,4},{6,7},{7,6},{8,9},{9,8},{10,11... | collective-permute-start | bytes 393224 | tf_op jit(solution)/shard_map/ppermute | solution.py:28
  213.2 1.3 collective-permute-done.5
  214.5 1.1 fusion.104
  215.6 2.0 collective-permute-start.7
  217.5 0.7 fusion.84
  218.2 4.0 %collective-permute-done.7 = bf16[128,4,128]{2,0,1:T(8,128)(2,1)S(1)} collective-permute-done((bf16[128,4,128]{2,0,1:T(8,128)(2,1)S(1)}, bf16[128,4,128]{2,0,1:T(8,128)(2,1)S(1)}, u32[]{:S(2)}, u32[]{:S(2)}) %collective-permute-start.7) | collective-permute-done | bytes 131104 | tf_op jit(solution)/shard_map/ppermute | solution.py:28
  222.2 1.2 fusion.8
  223.4 6.5 %all-to-all-start = ((bf16[16,8,2048]{2,1,0:T(8,128)(2,1)}), bf16[16,8,2048]{2,1,0:T(8,128)(2,1)S(1)}, u32[]{:S(2)}, u32[]{:S(2)}) async-start(bf16[16,8,2048]{2,1,0:T(8,128)(2,1)} %fusion.8), calls=%async_computation | async-start | bytes 1048576 | tf_op jit(solution)/shard_map/all_to_all | solution.py:17
  230.0 0.8 fusion.105
  230.8 0.8 fusion.106
  231.6 1.5 pad_maximum_fusion.1
  233.2 13.9 %all-to-all-done = bf16[16,8,2048]{2,1,0:T(8,128)(2,1)S(1)} async-done(((bf16[16,8,2048]{2,1,0:T(8,128)(2,1)}), bf16[16,8,2048]{2,1,0:T(8,128)(2,1)S(1)}, u32[]{:S(2)}, u32[]{:S(2)}) %all-to-all-start) | async-done | bytes 524320 | tf_op jit(solution)/shard_map/all_to_all | solution.py:17
  247.6 16.0 %all_gather.21 = bf16[128,2048]{1,0:T(8,128)(2,1)S(1)} all-gather(bf16[8,2048]{1,0:T(8,128)(2,1)S(1)} %multiply_convert_fusion.1), channel_id=1, replica_groups=mesh['grp'=2,'sp'=16,'tp'=16] {'tp'}, dimensions={0}, use_global_device_ids=true | all-gather | bytes 557056 | tf_op jit(solution)/shard_map/all_gather | solution.py:52
  263.6 0.4 convolution_convert_fusion.5
  264.1 3.2 collective-permute-start.10
  267.8 2.1 collective-permute-start.11
  270.0 1.0 collective-permute-done.11
  271.1 0.6 fusion.9
  271.7 23.3 %all_to_all.15 = bf16[16,8,2048]{2,1,0:T(8,128)(2,1)S(1)} all-to-all(bf16[16,8,2048]{2,1,0:T(8,128)(2,1)S(1)} %fusion.9), channel_id=1, replica_groups=mesh['grp'=2,'sp'=16,'tp'=16] {'tp'}, dimensions={0} | all-to-all | bytes 1048576 | tf_op jit(solution)/shard_map/all_to_all | solution.py:17
  295.6 16.0 %all_gather.22 = bf16[128,2048]{1,0:T(8,128)(2,1)S(1)} all-gather(bf16[8,2048]{1,0:T(8,128)(2,1)S(1)} %multiply_convert_fusion), channel_id=1, replica_groups=mesh['grp'=2,'sp'=16,'tp'=16] {'tp'}, dimensions={0}, use_global_device_ids=true | all-gather | bytes 557056 | tf_op jit(solution)/shard_map/all_gather | solution.py:52
  311.9 2.1 collective-permute-start.12
  314.0 1.0 collective-permute-done.12
  315.1 2.2 collective-permute-start.13
  317.3 3.2 collective-permute-done.13
  320.5 2.7 multiply_reduce_fusion
  323.2 1.5 fusion.2
  324.7 3.0 collective-permute-start.14
  327.7 2.0 collective-permute-start.18
  329.7 2.2 collective-permute-start.16
  331.9 3.2 collective-permute-start.19
  335.1 1.2 collective-permute-done.19
  336.3 1.7 fusion.110
  338.0 3.9 %collective-permute-start.15 = (bf16[128,4,128]{2,0,1:T(8,128)(2,1)S(1)}, bf16[128,4,128]{2,0,1:T(8,128)(2,1)S(1)}, u32[]{:S(2)}, u32[]{:S(2)}) collective-permute-start(bf16[128,4,128]{2,0,1:T(8,128)(2,1)S(1)} %get-tuple-element.51), channel_id=1, source_target_pairs={{0,1},{1,0},{2,3},{3,2},{4,5},{5,4},{6,7},{7,6},{8,9},{9,8},{10,11... | collective-permute-start | bytes 393224 | tf_op jit(solution)/shard_map/ppermute | solution.py:28
  341.9 0.9 collective-permute-done.15
  343.0 3.2 collective-permute-start.17
  346.2 3.4 collective-permute-done.17
  349.6 0.4 fusion.10
  350.0 23.3 %all_to_all.16 = bf16[16,8,2048]{2,1,0:T(8,128)(2,1)S(1)} all-to-all(bf16[16,8,2048]{2,1,0:T(8,128)(2,1)S(1)} %fusion.10), channel_id=1, replica_groups=mesh['grp'=2,'sp'=16,'tp'=16] {'tp'}, dimensions={0} | all-to-all | bytes 1048576 | tf_op jit(solution)/shard_map/all_to_all | solution.py:17
  373.5 0.7 multiply_add_fusion.2
  (92 shorter events, 3.9 us)
Async XLA Ops:
  6.5 264.6 %copy-start = (bf16[176,2048]{1,0:T(8,128)(2,1)S(1)}, bf16[176,2048]{1,0:T(8,128)(2,1)}, u32[]{:S(2)}) copy-start(bf16[176,2048]{1,0:T(8,128)(2,1)} %param.33) | copy-start | bytes 2162692
  6.6 101.9 %copy-start.1 = (bf16[8,2048]{1,0:T(8,128)(2,1)S(1)}, bf16[8,2048]{1,0:T(8,128)(2,1)}, u32[]{:S(2)}) copy-start(bf16[8,2048]{1,0:T(8,128)(2,1)} %param.20) | copy-start | bytes 98308
  6.6 102.0 %copy-start.11 = (f32[2048]{0:T(1024)S(1)}, f32[2048]{0:T(1024)}, u32[]{:S(2)}) copy-start(f32[2048]{0:T(1024)} %param.23) | copy-start | bytes 24580
  6.6 120.8 %copy-start.4 = (bf16[2048,128]{1,0:T(8,128)(2,1)S(1)}, bf16[2048,128]{1,0:T(8,128)(2,1)}, u32[]{:S(2)}) copy-start(bf16[2048,128]{1,0:T(8,128)(2,1)} %param.24) | copy-start | bytes 1572868
  6.6 86.4 %all-gather.4.cloned.1.call-start = ((), (), s32[]{:S(2)}) async-start(), calls=%async_computation.3 | async-start | bytes 4456448 | tf_op jit(solution)/shard_map/all_gather | solution.py:70
  9.7 168.6 %all-gather.6.cloned.1.call-start = ((), (), s32[]{:S(2)}) async-start(), calls=%async_computation.4 | async-start | bytes 2228224 | tf_op jit(solution)/shard_map/all_gather | solution.py:33
  96.9 3.3 collective-permute-start.2
  100.2 6.7 %collective-permute-start.3 = (bf16[2,128,256]{2,1,0:T(8,128)(2,1)S(1)}, bf16[2,128,256]{2,1,0:T(8,128)(2,1)S(1)}, u32[]{:S(2)}, u32[]{:S(2)}) collective-permute-start(bf16[2,128,256]{2,1,0:T(8,128)(2,1)S(1)} %get-tuple-element.30), channel_id=1, source_target_pairs={{0,2},{2,0},{1,3},{3,1},{4,6},{6,4},{5,7},{7,5},{8,10},{10,8},{9,1... | collective-permute-start | bytes 393224 | tf_op jit(solution)/shard_map/ppermute | solution.py:28
  127.7 3.1 collective-permute-start
  130.9 5.5 %collective-permute-start.1 = (bf16[128,256]{0,1:T(8,128)(2,1)S(1)}, bf16[128,256]{0,1:T(8,128)(2,1)S(1)}, u32[]{:S(2)}, u32[]{:S(2)}) collective-permute-start(bf16[128,256]{0,1:T(8,128)(2,1)S(1)} %maximum_select_fusion.7), channel_id=1, source_target_pairs={{0,2},{2,0},{1,3},{3,1},{4,6},{6,4},{5,7},{7,5},{8,10},{10,8},{9,1... | collective-permute-start | bytes 196616 | tf_op jit(solution)/shard_map/ppermute | solution.py:28
  178.3 28.5 %copy-start.9 = (bf16[256,4096]{1,0:T(8,128)(2,1)S(1)}, bf16[256,4096]{1,0:T(8,128)(2,1)}, u32[]{:S(2)}) copy-start(bf16[256,4096]{1,0:T(8,128)(2,1)} %all-gather.6.cloned.1.call-done) | copy-start | bytes 6291460
  181.1 41.1 %copy-start.5 = (bf16[128,2048]{1,0:T(8,128)(2,1)S(1)}, bf16[128,2048]{1,0:T(8,128)(2,1)}, u32[]{:S(2)}) copy-start(bf16[128,2048]{1,0:T(8,128)(2,1)} %param.26) | copy-start | bytes 1572868
  182.6 64.7 %copy-start.10 = (f32[2048]{0:T(1024)S(1)}, f32[2048]{0:T(1024)}, u32[]{:S(2)}) copy-start(f32[2048]{0:T(1024)} %param.27) | copy-start | bytes 24580
  182.6 64.9 %copy-start.12 = (f32[2048]{0:T(1024)S(1)}, f32[2048]{0:T(1024)}, u32[]{:S(2)}) copy-start(f32[2048]{0:T(1024)} %param.28) | copy-start | bytes 24580
  182.6 81.0 %copy-start.2 = (bf16[2048,176]{0,1:T(8,128)(2,1)S(1)}, bf16[2048,176]{0,1:T(8,128)(2,1)}, u32[]{:S(2)}) copy-start(bf16[2048,176]{0,1:T(8,128)(2,1)} %param.29) | copy-start | bytes 2162692
  182.6 84.7 %copy-start.3 = (bf16[2048,176]{0,1:T(8,128)(2,1)S(1)}, bf16[2048,176]{0,1:T(8,128)(2,1)}, u32[]{:S(2)}) copy-start(bf16[2048,176]{0,1:T(8,128)(2,1)} %param.30) | copy-start | bytes 2162692
  182.7 15.7 %collective-permute-start.4 = (bf16[128,4]{0,1:T(4,128)(2,1)S(1)}, bf16[128,4]{0,1:T(4,128)(2,1)S(1)}, u32[]{:S(2)}, u32[]{:S(2)}) collective-permute-start(bf16[128,4]{0,1:T(4,128)(2,1)S(1)} %get-tuple-element.43), channel_id=1, source_target_pairs={{0,1},{1,0},{2,3},{3,2},{4,5},{5,4},{6,7},{7,6},{8,9},{9,8},{10,11... | collective-permute-start | bytes 3080 | tf_op jit(solution)/shard_map/ppermute | solution.py:28
  196.4 5.5 %collective-permute-start.8 = (bf16[128,4]{0,1:T(4,128)(2,1)S(1)}, bf16[128,4]{0,1:T(4,128)(2,1)S(1)}, u32[]{:S(2)}, u32[]{:S(2)}) collective-permute-start(bf16[128,4]{0,1:T(4,128)(2,1)S(1)} %get-tuple-element.44), channel_id=1, source_target_pairs={{0,1},{1,0},{2,3},{3,2},{4,5},{5,4},{6,7},{7,6},{8,9},{9,8},{10,11... | collective-permute-start | bytes 3080 | tf_op jit(solution)/shard_map/ppermute | solution.py:28
  198.4 5.5 %collective-permute-start.6 = (bf16[128,4]{0,1:T(4,128)(2,1)S(1)}, bf16[128,4]{0,1:T(4,128)(2,1)S(1)}, u32[]{:S(2)}, u32[]{:S(2)}) collective-permute-start(bf16[128,4]{0,1:T(4,128)(2,1)S(1)} %fusion.82), channel_id=1, source_target_pairs={{0,2},{2,0},{1,3},{3,1},{4,6},{6,4},{5,7},{7,5},{8,10},{10,8},{9,1... | collective-permute-start | bytes 3080 | tf_op jit(solution)/shard_map/ppermute | solution.py:28
  201.9 4.3 %collective-permute-start.9 = (bf16[128,4]{0,1:T(4,128)(2,1)S(1)}, bf16[128,4]{0,1:T(4,128)(2,1)S(1)}, u32[]{:S(2)}, u32[]{:S(2)}) collective-permute-start(bf16[128,4]{0,1:T(4,128)(2,1)S(1)} %get-tuple-element.19), channel_id=1, source_target_pairs={{0,2},{2,0},{1,3},{3,1},{4,6},{6,4},{5,7},{7,5},{8,10},{10,8},{9,1... | collective-permute-start | bytes 3080 | tf_op jit(solution)/shard_map/ppermute | solution.py:28
  206.8 88.4 %copy-start.13 = (f32[2048]{0:T(1024)S(1)}, f32[2048]{0:T(1024)}, u32[]{:S(2)}) copy-start(f32[2048]{0:T(1024)} %param.34) | copy-start | bytes 24580
  206.8 88.7 %copy-start.15 = (f32[2048]{0:T(1024)S(1)}, f32[2048]{0:T(1024)}, u32[]{:S(2)}) copy-start(f32[2048]{0:T(1024)} %param.35) | copy-start | bytes 24580
  209.2 102.4 %copy-start.6 = (bf16[2048,128]{1,0:T(8,128)(2,1)S(1)}, bf16[2048,128]{1,0:T(8,128)(2,1)}, u32[]{:S(2)}) copy-start(bf16[2048,128]{1,0:T(8,128)(2,1)} %param.36) | copy-start | bytes 1572868
  209.2 5.3 %collective-permute-start.5 = (bf16[128,4,128]{2,0,1:T(8,128)(2,1)}, bf16[128,4,128]{2,0,1:T(8,128)(2,1)}, u32[]{:S(2)}, u32[]{:S(2)}) collective-permute-start(bf16[128,4,128]{2,0,1:T(8,128)(2,1)} %get-tuple-element.47), channel_id=1, source_target_pairs={{0,1},{1,0},{2,3},{3,2},{4,5},{5,4},{6,7},{7,6},{8,9},{9,8},{10,11... | collective-permute-start | bytes 393224 | tf_op jit(solution)/shard_map/ppermute | solution.py:28
  215.6 6.6 %collective-permute-start.7 = (bf16[128,4,128]{2,0,1:T(8,128)(2,1)S(1)}, bf16[128,4,128]{2,0,1:T(8,128)(2,1)S(1)}, u32[]{:S(2)}, u32[]{:S(2)}) collective-permute-start(bf16[128,4,128]{2,0,1:T(8,128)(2,1)S(1)} %get-tuple-element.23), channel_id=1, source_target_pairs={{0,2},{2,0},{1,3},{3,1},{4,6},{6,4},{5,7},{7,5},{8,10},{10,8},{9,1... | collective-permute-start | bytes 393224 | tf_op jit(solution)/shard_map/ppermute | solution.py:28
  223.4 23.7 %all-to-all-start = ((bf16[16,8,2048]{2,1,0:T(8,128)(2,1)}), bf16[16,8,2048]{2,1,0:T(8,128)(2,1)S(1)}, u32[]{:S(2)}, u32[]{:S(2)}) async-start(bf16[16,8,2048]{2,1,0:T(8,128)(2,1)} %fusion.8), calls=%async_computation | async-start | bytes 1048576 | tf_op jit(solution)/shard_map/all_to_all | solution.py:17
  229.9 87.4 %all-gather.8.cloned.1.call-start = ((), (), s32[]{:S(2)}) async-start(), calls=%async_computation.5 | async-start | bytes 2228224 | tf_op jit(solution)/shard_map/all_gather | solution.py:33
  264.1 5.8 %collective-permute-start.10 = (bf16[2,176]{0,1:T(8,128)(2,1)S(1)}, bf16[2,176]{0,1:T(8,128)(2,1)S(1)}, u32[]{:S(2)}, u32[]{:S(2)}) collective-permute-start(bf16[2,176]{0,1:T(8,128)(2,1)S(1)} %slice.122), channel_id=1, source_target_pairs={{0,16},{16,32},{32,48},{48,64},{64,80},{80,96},{96,112},{112,128},... | collective-permute-start | bytes 2120 | tf_op jit(solution)/shard_map/ppermute | solution.py:43
  267.8 3.2 collective-permute-start.11
  311.9 3.1 collective-permute-start.12
  315.1 5.4 %collective-permute-start.13 = (bf16[128,256]{0,1:T(8,128)(2,1)S(1)}, bf16[128,256]{0,1:T(8,128)(2,1)S(1)}, u32[]{:S(2)}, u32[]{:S(2)}) collective-permute-start(bf16[128,256]{0,1:T(8,128)(2,1)S(1)} %maximum_select_fusion.9), channel_id=1, source_target_pairs={{0,2},{2,0},{1,3},{3,1},{4,6},{6,4},{5,7},{7,5},{8,10},{10,8},{9,1... | collective-permute-start | bytes 196616 | tf_op jit(solution)/shard_map/ppermute | solution.py:28
  320.5 15.8 %copy-start.8 = (bf16[256,4096]{1,0:T(8,128)(2,1)S(1)}, bf16[256,4096]{1,0:T(8,128)(2,1)}, u32[]{:S(2)}) copy-start(bf16[256,4096]{1,0:T(8,128)(2,1)} %all-gather.8.cloned.1.call-done) | copy-start | bytes 6291460
  323.2 26.4 %copy-start.7 = (bf16[128,2048]{1,0:T(8,128)(2,1)S(1)}, bf16[128,2048]{1,0:T(8,128)(2,1)}, u32[]{:S(2)}) copy-start(bf16[128,2048]{1,0:T(8,128)(2,1)} %param.38) | copy-start | bytes 1572868
  324.7 48.8 %copy-start.14 = (f32[2048]{0:T(1024)S(1)}, f32[2048]{0:T(1024)}, u32[]{:S(2)}) copy-start(f32[2048]{0:T(1024)} %param.39) | copy-start | bytes 24580
  324.7 4.9 %collective-permute-start.14 = (bf16[128,4]{0,1:T(4,128)(2,1)S(1)}, bf16[128,4]{0,1:T(4,128)(2,1)S(1)}, u32[]{:S(2)}, u32[]{:S(2)}) collective-permute-start(bf16[128,4]{0,1:T(4,128)(2,1)S(1)} %get-tuple-element.40), channel_id=1, source_target_pairs={{0,1},{1,0},{2,3},{3,2},{4,5},{5,4},{6,7},{7,6},{8,9},{9,8},{10,11... | collective-permute-start | bytes 3080 | tf_op jit(solution)/shard_map/ppermute | solution.py:28
  327.7 4.2 %collective-permute-start.18 = (bf16[128,4]{0,1:T(4,128)(2,1)S(1)}, bf16[128,4]{0,1:T(4,128)(2,1)S(1)}, u32[]{:S(2)}, u32[]{:S(2)}) collective-permute-start(bf16[128,4]{0,1:T(4,128)(2,1)S(1)} %get-tuple-element.41), channel_id=1, source_target_pairs={{0,1},{1,0},{2,3},{3,2},{4,5},{5,4},{6,7},{7,6},{8,9},{9,8},{10,11... | collective-permute-start | bytes 3080 | tf_op jit(solution)/shard_map/ppermute | solution.py:28
  329.7 5.4 %collective-permute-start.16 = (bf16[128,4]{0,1:T(4,128)(2,1)S(1)}, bf16[128,4]{0,1:T(4,128)(2,1)S(1)}, u32[]{:S(2)}, u32[]{:S(2)}) collective-permute-start(bf16[128,4]{0,1:T(4,128)(2,1)S(1)} %fusion.83), channel_id=1, source_target_pairs={{0,2},{2,0},{1,3},{3,1},{4,6},{6,4},{5,7},{7,5},{8,10},{10,8},{9,1... | collective-permute-start | bytes 3080 | tf_op jit(solution)/shard_map/ppermute | solution.py:28
  331.9 4.3 %collective-permute-start.19 = (bf16[128,4]{0,1:T(4,128)(2,1)S(1)}, bf16[128,4]{0,1:T(4,128)(2,1)S(1)}, u32[]{:S(2)}, u32[]{:S(2)}) collective-permute-start(bf16[128,4]{0,1:T(4,128)(2,1)S(1)} %get-tuple-element.8), channel_id=1, source_target_pairs={{0,2},{2,0},{1,3},{3,1},{4,6},{6,4},{5,7},{7,5},{8,10},{10,8},{9,1... | collective-permute-start | bytes 3080 | tf_op jit(solution)/shard_map/ppermute | solution.py:28
  338.0 4.8 %collective-permute-start.15 = (bf16[128,4,128]{2,0,1:T(8,128)(2,1)S(1)}, bf16[128,4,128]{2,0,1:T(8,128)(2,1)S(1)}, u32[]{:S(2)}, u32[]{:S(2)}) collective-permute-start(bf16[128,4,128]{2,0,1:T(8,128)(2,1)S(1)} %get-tuple-element.51), channel_id=1, source_target_pairs={{0,1},{1,0},{2,3},{3,2},{4,5},{5,4},{6,7},{7,6},{8,9},{9,8},{10,11... | collective-permute-start | bytes 393224 | tf_op jit(solution)/shard_map/ppermute | solution.py:28
  343.0 6.6 %collective-permute-start.17 = (bf16[128,4,128]{2,0,1:T(8,128)(2,1)S(1)}, bf16[128,4,128]{2,0,1:T(8,128)(2,1)S(1)}, u32[]{:S(2)}, u32[]{:S(2)}) collective-permute-start(bf16[128,4,128]{2,0,1:T(8,128)(2,1)S(1)} %get-tuple-element.12), channel_id=1, source_target_pairs={{0,2},{2,0},{1,3},{3,1},{4,6},{6,4},{5,7},{7,5},{8,10},{10,8},{9,1... | collective-permute-start | bytes 393224 | tf_op jit(solution)/shard_map/ppermute | solution.py:28
Sparse Core Ops, SparseCore 0:
  9.8 83.0 all-gather.3
  108.6 69.7 all-gather.5
  233.3 66.6 all-gather.7
where the time goes:
time: 382 us; the launch traced here: 381 us
  waiting for transfers between devices  167 us (44%)
  blocking collectives  97.2 us (25%)
  starting transfers between devices  70 us (18%)
  matrix products  16.9 us (4%)
  between operations  13.8 us (4%)
  other arithmetic  12.8 us (3%)
    all_gather x1, waiting for transfers between devices, key_columns(): lax.all_gather(source_rows, 'tp', axis=0, tiled=True)  83.2 us
    ppermute x18, starting transfers between devices, swapped(): return lax.ppermute(block, axis, route)  57.9 us
    all_gather x3, blocking collectives, project_rows(): shard_rows = lax.all_gather(rows_here, 'tp', axis=0, tiled=True)  50.6 us
    all_to_all x2, blocking collectives, sent_and_summed(): lax.all_to_all(parts, axis, split_axis=0, concat_axis=0, tiled=True)  46.6 us
    all_gather x2, waiting for transfers between devices, in_one_piece(): result, at, done = (lax.all_gather(both, axis, axis=dim, tiled=True), 0, [])  42 us
    ppermute x18, waiting for transfers between devices, swapped(): return lax.ppermute(block, axis, route)  26.6 us
    all_to_all x1, waiting for transfers between devices, sent_and_summed(): lax.all_to_all(parts, axis, split_axis=0, concat_axis=0, tiled=True)  13.9 us
  transfers between devices with their start and end apart: 24, of which 16 were waited for; matrix products, arithmetic and copies ran while one was open for 2% of the time, Pallas kernels for 0%

commit v1 on v0

--- a/solution.py
+++ b/solution.py
@@ -5,6 +5,14 @@
 
 HEAD = 128
 KVH = 4
+
+
+def supply_all_edge(arr):
+    buffers = []
+    extent = lax.axis_size("tp")
+    for ix in range(arr.ndim):
+        buffers.append(extent if ix == 0 else 1)
+    return lax.all_to_all(jnp.tile(arr, buffers), "tp", concat_axis=0, tiled=True, split_axis=0)
 
 
 def in_blocks(array, dim, size):
@@ -66,10 +74,7 @@
 def key_columns(source_rows, keyval_first, keyval_second):
     both_layers = jnp.concatenate([keyval_first, keyval_second], axis=1)
     columns = jnp.einsum(
-        "rd,dc->cr",
-        lax.all_gather(source_rows, "tp", axis=0, tiled=True),
-        both_layers,
-        preferred_element_type=jnp.float32,
+        "rd,dc->cr", supply_all_edge(source_rows), both_layers, preferred_element_type=jnp.float32
     ).astype(jnp.bfloat16)
     column_count = keyval_first.shape[1]
     stacked = columns.reshape(2, column_count, columns.shape[1])

time: 382 us -> 436 us (1.14)
  starting transfers between devices: 70 us -> 116 us
  waiting for transfers between devices: 167 us -> 173 us
    all_to_all x0 -> x1, waiting for transfers between devices: none -> 93.6 us  [supply_all_edge(): lax.all_to_all(jnp.tile(arr, buffers), 'tp', concat_axis=0, tiled=True, s...]
    all_gather x1 -> x0, waiting for transfers between devices: 83.2 us -> none  [key_columns(): lax.all_gather(source_rows, 'tp', axis=0, tiled=True)]
    all_to_all x0 -> x1, starting transfers between devices: none -> 45.8 us  [supply_all_edge(): lax.all_to_all(jnp.tile(arr, buffers), 'tp', concat_axis=0, tiled=True, s...]
    all_gather x2, waiting for transfers between devices: 42 us -> 37.6 us  [in_one_piece(): result, at, done = (lax.all_gather(both, axis, axis=dim, tiled=True), 0, [])]
where the time goes in v1:
time: 436 us; the launch traced here: 434 us
  waiting for transfers between devices  173 us (40%)
  starting transfers between devices  116 us (27%)
  blocking collectives  96.6 us (22%)
  matrix products  16.8 us (4%)
  between operations  14.1 us (3%)
  other arithmetic  12.1 us (3%)
  local copies, waits for them, and re-layouts  5.74 us (1%)
    all_to_all x1, waiting for transfers between devices, supply_all_edge(): lax.all_to_all(jnp.tile(arr, buffers), 'tp', concat_axis=0, tiled=True, s...  93.6 us
    ppermute x18, starting transfers between devices, swapped(): return lax.ppermute(block, axis, route)  57.8 us
    all_gather x3, blocking collectives, project_rows(): shard_rows = lax.all_gather(rows_here, 'tp', axis=0, tiled=True)  50 us
    all_to_all x2, blocking collectives, sent_and_summed(): lax.all_to_all(parts, axis, split_axis=0, concat_axis=0, tiled=True)  46.6 us
    all_to_all x1, starting transfers between devices, supply_all_edge(): lax.all_to_all(jnp.tile(arr, buffers), 'tp', concat_axis=0, tiled=True, s...  45.8 us
    all_gather x2, waiting for transfers between devices, in_one_piece(): result, at, done = (lax.all_gather(both, axis, axis=dim, tiled=True), 0, [])  37.6 us
    ppermute x18, waiting for transfers between devices, swapped(): return lax.ppermute(block, axis, route)  26.7 us
    all_to_all x1, waiting for transfers between devices, sent_and_summed(): lax.all_to_all(parts, axis, split_axis=0, concat_axis=0, tiled=True)  13.9 us
  transfers between devices with their start and end apart: 24, of which 16 were waited for; matrix products, arithmetic and copies ran while one was open for 2% of the time, Pallas kernels for 0%

profile of v1, /device:TPU:65, one launch (start us, length us, event | category | flops | bytes accessed | tf_op | source)
XLA Modules:
  0.0 434.4 jit_solution(17654874919762111300)
XLA Ops:
  6.6 1.2 fusion.19
  7.8 1.1 fusion.21
  8.9 2.5 tile.2
  11.4 45.8 %all-to-all-start = ((bf16[16,64,2048]{2,1,0:T(8,128)(2,1)}), bf16[16,64,2048]{2,1,0:T(8,128)(2,1)}, u32[]{:S(2)}, u32[]{:S(2)}) async-start(bf16[16,64,2048]{2,1,0:T(8,128)(2,1)} %tile.2), calls=%async_computation | async-start | bytes 8388608 | tf_op jit(solution)/shard_map/all_to_all | solution.py:15
  57.3 93.6 %all-to-all-done = bf16[16,64,2048]{2,1,0:T(8,128)(2,1)} async-done(((bf16[16,64,2048]{2,1,0:T(8,128)(2,1)}), bf16[16,64,2048]{2,1,0:T(8,128)(2,1)}, u32[]{:S(2)}, u32[]{:S(2)}) %all-to-all-start) | async-done | bytes 4194336 | tf_op jit(solution)/shard_map/all_to_all | solution.py:15
  151.0 3.7 convolution_convert_fusion.3
  154.7 2.9 collective-permute-start.2
  157.6 0.9 collective-permute-done.2
  158.7 2.0 collective-permute-start.3
  160.6 4.7 %collective-permute-done.3 = bf16[2,128,256]{2,1,0:T(8,128)(2,1)S(1)} collective-permute-done((bf16[2,128,256]{2,1,0:T(8,128)(2,1)S(1)}, bf16[2,128,256]{2,1,0:T(8,128)(2,1)S(1)}, u32[]{:S(2)}, u32[]{:S(2)}) %collective-permute-start.3) | collective-permute-done | bytes 131104 | tf_op jit(solution)/shard_map/ppermute | solution.py:36
  165.4 0.7 slice_bitcast_fusion.9
  166.1 0.7 pad_maximum_fusion
  167.0 18.1 %all_gather.15 = bf16[128,2048]{1,0:T(8,128)(2,1)S(1)} all-gather(bf16[8,2048]{1,0:T(8,128)(2,1)S(1)} %fusion.52), channel_id=1, replica_groups=mesh['grp'=2,'sp'=16,'tp'=16] {'tp'}, dimensions={0}, use_global_device_ids=true | all-gather | bytes 557056 | tf_op jit(solution)/shard_map/all_gather | solution.py:60
  185.5 2.1 collective-permute-start
  187.6 1.0 collective-permute-done
  188.6 2.2 collective-permute-start.1
  190.9 3.3 collective-permute-done.1
  194.1 37.5 %all-gather.3.cloned.1.call-done = bf16[256,4096]{1,0:T(8,128)(2,1)} async-done(((bf16[256,256]{1,0:T(8,128)(2,1)}), bf16[256,4096]{1,0:T(8,128)(2,1)}) %all-gather.3.cloned.1.call-update) | async-done | bytes 2097168 | tf_op jit(solution)/shard_map/all_gather | solution.py:41
  231.7 2.7 multiply_reduce_fusion.1
  234.4 1.5 fusion
  236.0 13.6 %collective-permute-start.4 = (bf16[128,4]{0,1:T(4,128)(2,1)S(1)}, bf16[128,4]{0,1:T(4,128)(2,1)S(1)}, u32[]{:S(2)}, u32[]{:S(2)}) collective-permute-start(bf16[128,4]{0,1:T(4,128)(2,1)S(1)} %get-tuple-element.43), channel_id=1, source_target_pairs={{0,1},{1,0},{2,3},{3,2},{4,5},{5,4},{6,7},{7,6},{8,9},{9,8},{10,11... | collective-permute-start | bytes 3080 | tf_op jit(solution)/shard_map/ppermute | solution.py:36
  249.6 2.0 collective-permute-start.8
  251.6 3.1 collective-permute-start.6
  254.8 2.2 collective-permute-start.9
  257.0 2.1 collective-permute-done.9
  259.1 0.6 multiply_add_fusion.6
  259.7 2.3 fusion.109
  262.0 4.0 collective-permute-start.5
  266.0 1.3 collective-permute-done.5
  267.3 1.1 fusion.104
  268.4 2.2 collective-permute-start.7
  270.6 0.7 fusion.84
  271.3 3.7 collective-permute-done.7
  275.1 1.2 fusion.8
  276.2 7.0 %all-to-all-start.1 = ((bf16[16,8,2048]{2,1,0:T(8,128)(2,1)}), bf16[16,8,2048]{2,1,0:T(8,128)(2,1)S(1)}, u32[]{:S(2)}, u32[]{:S(2)}) async-start(bf16[16,8,2048]{2,1,0:T(8,128)(2,1)} %fusion.8), calls=%async_computation.1 | async-start | bytes 1048576 | tf_op jit(solution)/shard_map/all_to_all | solution.py:25
  283.3 0.8 fusion.105
  284.1 0.8 fusion.106
  284.9 1.5 pad_maximum_fusion.1
  286.5 13.9 %all-to-all-done.1 = bf16[16,8,2048]{2,1,0:T(8,128)(2,1)S(1)} async-done(((bf16[16,8,2048]{2,1,0:T(8,128)(2,1)}), bf16[16,8,2048]{2,1,0:T(8,128)(2,1)S(1)}, u32[]{:S(2)}, u32[]{:S(2)}) %all-to-all-start.1) | async-done | bytes 524320 | tf_op jit(solution)/shard_map/all_to_all | solution.py:25
  301.0 16.0 %all_gather.17 = bf16[128,2048]{1,0:T(8,128)(2,1)S(1)} all-gather(bf16[8,2048]{1,0:T(8,128)(2,1)S(1)} %multiply_convert_fusion.1), channel_id=1, replica_groups=mesh['grp'=2,'sp'=16,'tp'=16] {'tp'}, dimensions={0}, use_global_device_ids=true | all-gather | bytes 557056 | tf_op jit(solution)/shard_map/all_gather | solution.py:60
  317.4 3.0 collective-permute-start.10
  320.9 2.5 collective-permute-start.11
  323.5 0.8 collective-permute-done.11
  324.5 0.6 fusion.9
  325.1 23.3 %all_to_all.24 = bf16[16,8,2048]{2,1,0:T(8,128)(2,1)S(1)} all-to-all(bf16[16,8,2048]{2,1,0:T(8,128)(2,1)S(1)} %fusion.9), channel_id=1, replica_groups=mesh['grp'=2,'sp'=16,'tp'=16] {'tp'}, dimensions={0} | all-to-all | bytes 1048576 | tf_op jit(solution)/shard_map/all_to_all | solution.py:25
  348.9 16.0 %all_gather.18 = bf16[128,2048]{1,0:T(8,128)(2,1)S(1)} all-gather(bf16[8,2048]{1,0:T(8,128)(2,1)S(1)} %multiply_convert_fusion), channel_id=1, replica_groups=mesh['grp'=2,'sp'=16,'tp'=16] {'tp'}, dimensions={0}, use_global_device_ids=true | all-gather | bytes 557056 | tf_op jit(solution)/shard_map/all_gather | solution.py:60
  365.2 2.1 collective-permute-start.12
  367.4 1.0 collective-permute-done.12
  368.4 2.2 collective-permute-start.13
  370.6 3.2 collective-permute-done.13
  373.8 2.7 multiply_reduce_fusion
  376.6 1.5 fusion.2
  378.1 3.0 collective-permute-start.14
  381.1 2.0 collective-permute-start.18
  383.0 2.2 collective-permute-start.16
  385.3 3.2 collective-permute-start.19
  388.4 1.2 collective-permute-done.19
  389.6 1.7 fusion.110
  391.3 3.9 collective-permute-start.15
  395.2 0.9 collective-permute-done.15
  396.4 3.2 collective-permute-start.17
  399.6 3.4 collective-permute-done.17
  403.4 23.3 %all_to_all.25 = bf16[16,8,2048]{2,1,0:T(8,128)(2,1)S(1)} all-to-all(bf16[16,8,2048]{2,1,0:T(8,128)(2,1)S(1)} %fusion.10), channel_id=1, replica_groups=mesh['grp'=2,'sp'=16,'tp'=16] {'tp'}, dimensions={0} | all-to-all | bytes 1048576 | tf_op jit(solution)/shard_map/all_to_all | solution.py:25
  426.9 0.7 multiply_add_fusion.2
  (96 shorter events, 4.5 us)
Async XLA Ops:
  6.5 317.9 %copy-start = (bf16[176,2048]{1,0:T(8,128)(2,1)S(1)}, bf16[176,2048]{1,0:T(8,128)(2,1)}, u32[]{:S(2)}) copy-start(bf16[176,2048]{1,0:T(8,128)(2,1)} %param.33) | copy-start | bytes 2162692
  6.6 144.4 %copy-start.11 = (bf16[2048,64]{0,1:T(8,128)(2,1)S(1)}, bf16[2048,64]{0,1:T(8,128)(2,1)}, u32[]{:S(2)}) copy-start(bf16[2048,64]{0,1:T(8,128)(2,1)} %param.25) | copy-start | bytes 786436
  6.6 144.4 %copy-start.10 = (bf16[2048,64]{0,1:T(8,128)(2,1)S(1)}, bf16[2048,64]{0,1:T(8,128)(2,1)}, u32[]{:S(2)}) copy-start(bf16[2048,64]{0,1:T(8,128)(2,1)} %param.37) | copy-start | bytes 786436
  11.4 155.4 %copy-start.1 = (bf16[8,2048]{1,0:T(8,128)(2,1)S(1)}, bf16[8,2048]{1,0:T(8,128)(2,1)}, u32[]{:S(2)}) copy-start(bf16[8,2048]{1,0:T(8,128)(2,1)} %param.20) | copy-start | bytes 98308
  11.4 155.5 %copy-start.13 = (f32[2048]{0:T(1024)S(1)}, f32[2048]{0:T(1024)}, u32[]{:S(2)}) copy-start(f32[2048]{0:T(1024)} %param.23) | copy-start | bytes 24580
  11.4 173.7 %copy-start.4 = (bf16[2048,128]{1,0:T(8,128)(2,1)S(1)}, bf16[2048,128]{1,0:T(8,128)(2,1)}, u32[]{:S(2)}) copy-start(bf16[2048,128]{1,0:T(8,128)(2,1)} %param.24) | copy-start | bytes 1572868
  11.4 139.6 %all-to-all-start = ((bf16[16,64,2048]{2,1,0:T(8,128)(2,1)}), bf16[16,64,2048]{2,1,0:T(8,128)(2,1)}, u32[]{:S(2)}, u32[]{:S(2)}) async-start(bf16[16,64,2048]{2,1,0:T(8,128)(2,1)} %tile.2), calls=%async_computation | async-start | bytes 8388608 | tf_op jit(solution)/shard_map/all_to_all | solution.py:15
  57.3 174.4 %all-gather.3.cloned.1.call-start = ((), (), s32[]{:S(2)}) async-start(), calls=%async_computation.4 | async-start | bytes 2228224 | tf_op jit(solution)/shard_map/all_gather | solution.py:41
  154.7 3.9 collective-permute-start.2
  158.7 6.6 %collective-permute-start.3 = (bf16[2,128,256]{2,1,0:T(8,128)(2,1)S(1)}, bf16[2,128,256]{2,1,0:T(8,128)(2,1)S(1)}, u32[]{:S(2)}, u32[]{:S(2)}) collective-permute-start(bf16[2,128,256]{2,1,0:T(8,128)(2,1)S(1)} %get-tuple-element.30), channel_id=1, source_target_pairs={{0,2},{2,0},{1,3},{3,1},{4,6},{6,4},{5,7},{7,5},{8,10},{10,8},{9,1... | collective-permute-start | bytes 393224 | tf_op jit(solution)/shard_map/ppermute | solution.py:36
  185.5 3.1 collective-permute-start
  188.6 5.5 %collective-permute-start.1 = (bf16[128,256]{0,1:T(8,128)(2,1)S(1)}, bf16[128,256]{0,1:T(8,128)(2,1)S(1)}, u32[]{:S(2)}, u32[]{:S(2)}) collective-permute-start(bf16[128,256]{0,1:T(8,128)(2,1)S(1)} %maximum_select_fusion.7), channel_id=1, source_target_pairs={{0,2},{2,0},{1,3},{3,1},{4,6},{6,4},{5,7},{7,5},{8,10},{10,8},{9,1... | collective-permute-start | bytes 196616 | tf_op jit(solution)/shard_map/ppermute | solution.py:36
  231.7 28.0 %copy-start.9 = (bf16[256,4096]{1,0:T(8,128)(2,1)S(1)}, bf16[256,4096]{1,0:T(8,128)(2,1)}, u32[]{:S(2)}) copy-start(bf16[256,4096]{1,0:T(8,128)(2,1)} %all-gather.3.cloned.1.call-done) | copy-start | bytes 6291460
  234.4 40.6 %copy-start.5 = (bf16[128,2048]{1,0:T(8,128)(2,1)S(1)}, bf16[128,2048]{1,0:T(8,128)(2,1)}, u32[]{:S(2)}) copy-start(bf16[128,2048]{1,0:T(8,128)(2,1)} %param.26) | copy-start | bytes 1572868
  235.9 64.7 %copy-start.12 = (f32[2048]{0:T(1024)S(1)}, f32[2048]{0:T(1024)}, u32[]{:S(2)}) copy-start(f32[2048]{0:T(1024)} %param.27) | copy-start | bytes 24580
  236.0 64.9 %copy-start.14 = (f32[2048]{0:T(1024)S(1)}, f32[2048]{0:T(1024)}, u32[]{:S(2)}) copy-start(f32[2048]{0:T(1024)} %param.28) | copy-start | bytes 24580
  236.0 81.0 %copy-start.2 = (bf16[2048,176]{0,1:T(8,128)(2,1)S(1)}, bf16[2048,176]{0,1:T(8,128)(2,1)}, u32[]{:S(2)}) copy-start(bf16[2048,176]{0,1:T(8,128)(2,1)} %param.29) | copy-start | bytes 2162692
  236.0 84.5 %copy-start.3 = (bf16[2048,176]{0,1:T(8,128)(2,1)S(1)}, bf16[2048,176]{0,1:T(8,128)(2,1)}, u32[]{:S(2)}) copy-start(bf16[2048,176]{0,1:T(8,128)(2,1)} %param.30) | copy-start | bytes 2162692
  236.0 15.6 %collective-permute-start.4 = (bf16[128,4]{0,1:T(4,128)(2,1)S(1)}, bf16[128,4]{0,1:T(4,128)(2,1)S(1)}, u32[]{:S(2)}, u32[]{:S(2)}) collective-permute-start(bf16[128,4]{0,1:T(4,128)(2,1)S(1)} %get-tuple-element.43), channel_id=1, source_target_pairs={{0,1},{1,0},{2,3},{3,2},{4,5},{5,4},{6,7},{7,6},{8,9},{9,8},{10,11... | collective-permute-start | bytes 3080 | tf_op jit(solution)/shard_map/ppermute | solution.py:36
  249.6 5.1 %collective-permute-start.8 = (bf16[128,4]{0,1:T(4,128)(2,1)S(1)}, bf16[128,4]{0,1:T(4,128)(2,1)S(1)}, u32[]{:S(2)}, u32[]{:S(2)}) collective-permute-start(bf16[128,4]{0,1:T(4,128)(2,1)S(1)} %get-tuple-element.44), channel_id=1, source_target_pairs={{0,1},{1,0},{2,3},{3,2},{4,5},{5,4},{6,7},{7,6},{8,9},{9,8},{10,11... | collective-permute-start | bytes 3080 | tf_op jit(solution)/shard_map/ppermute | solution.py:36
  251.6 5.4 %collective-permute-start.6 = (bf16[128,4]{0,1:T(4,128)(2,1)S(1)}, bf16[128,4]{0,1:T(4,128)(2,1)S(1)}, u32[]{:S(2)}, u32[]{:S(2)}) collective-permute-start(bf16[128,4]{0,1:T(4,128)(2,1)S(1)} %fusion.82), channel_id=1, source_target_pairs={{0,2},{2,0},{1,3},{3,1},{4,6},{6,4},{5,7},{7,5},{8,10},{10,8},{9,1... | collective-permute-start | bytes 3080 | tf_op jit(solution)/shard_map/ppermute | solution.py:36
  254.8 4.3 %collective-permute-start.9 = (bf16[128,4]{0,1:T(4,128)(2,1)S(1)}, bf16[128,4]{0,1:T(4,128)(2,1)S(1)}, u32[]{:S(2)}, u32[]{:S(2)}) collective-permute-start(bf16[128,4]{0,1:T(4,128)(2,1)S(1)} %get-tuple-element.19), channel_id=1, source_target_pairs={{0,2},{2,0},{1,3},{3,1},{4,6},{6,4},{5,7},{7,5},{8,10},{10,8},{9,1... | collective-permute-start | bytes 3080 | tf_op jit(solution)/shard_map/ppermute | solution.py:36
  259.7 88.9 %copy-start.15 = (f32[2048]{0:T(1024)S(1)}, f32[2048]{0:T(1024)}, u32[]{:S(2)}) copy-start(f32[2048]{0:T(1024)} %param.34) | copy-start | bytes 24580
  259.7 89.2 %copy-start.17 = (f32[2048]{0:T(1024)S(1)}, f32[2048]{0:T(1024)}, u32[]{:S(2)}) copy-start(f32[2048]{0:T(1024)} %param.35) | copy-start | bytes 24580
  262.0 102.9 %copy-start.6 = (bf16[2048,128]{1,0:T(8,128)(2,1)S(1)}, bf16[2048,128]{1,0:T(8,128)(2,1)}, u32[]{:S(2)}) copy-start(bf16[2048,128]{1,0:T(8,128)(2,1)} %param.36) | copy-start | bytes 1572868
  262.0 5.3 %collective-permute-start.5 = (bf16[128,4,128]{2,0,1:T(8,128)(2,1)}, bf16[128,4,128]{2,0,1:T(8,128)(2,1)}, u32[]{:S(2)}, u32[]{:S(2)}) collective-permute-start(bf16[128,4,128]{2,0,1:T(8,128)(2,1)} %get-tuple-element.47), channel_id=1, source_target_pairs={{0,1},{1,0},{2,3},{3,2},{4,5},{5,4},{6,7},{7,6},{8,9},{9,8},{10,11... | collective-permute-start | bytes 393224 | tf_op jit(solution)/shard_map/ppermute | solution.py:36
  268.4 6.6 %collective-permute-start.7 = (bf16[128,4,128]{2,0,1:T(8,128)(2,1)S(1)}, bf16[128,4,128]{2,0,1:T(8,128)(2,1)S(1)}, u32[]{:S(2)}, u32[]{:S(2)}) collective-permute-start(bf16[128,4,128]{2,0,1:T(8,128)(2,1)S(1)} %get-tuple-element.23), channel_id=1, source_target_pairs={{0,2},{2,0},{1,3},{3,1},{4,6},{6,4},{5,7},{7,5},{8,10},{10,8},{9,1... | collective-permute-start | bytes 393224 | tf_op jit(solution)/shard_map/ppermute | solution.py:36
  276.2 24.2 %all-to-all-start.1 = ((bf16[16,8,2048]{2,1,0:T(8,128)(2,1)}), bf16[16,8,2048]{2,1,0:T(8,128)(2,1)S(1)}, u32[]{:S(2)}, u32[]{:S(2)}) async-start(bf16[16,8,2048]{2,1,0:T(8,128)(2,1)} %fusion.8), calls=%async_computation.1 | async-start | bytes 1048576 | tf_op jit(solution)/shard_map/all_to_all | solution.py:25
  283.3 87.4 %all-gather.5.cloned.1.call-start = ((), (), s32[]{:S(2)}) async-start(), calls=%async_computation.5 | async-start | bytes 2228224 | tf_op jit(solution)/shard_map/all_gather | solution.py:41
  317.4 6.0 %collective-permute-start.10 = (bf16[2,176]{0,1:T(8,128)(2,1)S(1)}, bf16[2,176]{0,1:T(8,128)(2,1)S(1)}, u32[]{:S(2)}, u32[]{:S(2)}) collective-permute-start(bf16[2,176]{0,1:T(8,128)(2,1)S(1)} %slice.122), channel_id=1, source_target_pairs={{0,16},{16,32},{32,48},{48,64},{64,80},{80,96},{96,112},{112,128},... | collective-permute-start | bytes 2120 | tf_op jit(solution)/shard_map/ppermute | solution.py:51
  320.9 3.4 collective-permute-start.11
  365.2 3.1 collective-permute-start.12
  368.4 5.4 %collective-permute-start.13 = (bf16[128,256]{0,1:T(8,128)(2,1)S(1)}, bf16[128,256]{0,1:T(8,128)(2,1)S(1)}, u32[]{:S(2)}, u32[]{:S(2)}) collective-permute-start(bf16[128,256]{0,1:T(8,128)(2,1)S(1)} %maximum_select_fusion.9), channel_id=1, source_target_pairs={{0,2},{2,0},{1,3},{3,1},{4,6},{6,4},{5,7},{7,5},{8,10},{10,8},{9,1... | collective-permute-start | bytes 196616 | tf_op jit(solution)/shard_map/ppermute | solution.py:36
  373.8 15.8 %copy-start.8 = (bf16[256,4096]{1,0:T(8,128)(2,1)S(1)}, bf16[256,4096]{1,0:T(8,128)(2,1)}, u32[]{:S(2)}) copy-start(bf16[256,4096]{1,0:T(8,128)(2,1)} %all-gather.5.cloned.1.call-done) | copy-start | bytes 6291460
  376.6 26.4 %copy-start.7 = (bf16[128,2048]{1,0:T(8,128)(2,1)S(1)}, bf16[128,2048]{1,0:T(8,128)(2,1)}, u32[]{:S(2)}) copy-start(bf16[128,2048]{1,0:T(8,128)(2,1)} %param.38) | copy-start | bytes 1572868
  378.1 48.8 %copy-start.16 = (f32[2048]{0:T(1024)S(1)}, f32[2048]{0:T(1024)}, u32[]{:S(2)}) copy-start(f32[2048]{0:T(1024)} %param.39) | copy-start | bytes 24580
  378.1 4.9 %collective-permute-start.14 = (bf16[128,4]{0,1:T(4,128)(2,1)S(1)}, bf16[128,4]{0,1:T(4,128)(2,1)S(1)}, u32[]{:S(2)}, u32[]{:S(2)}) collective-permute-start(bf16[128,4]{0,1:T(4,128)(2,1)S(1)} %get-tuple-element.40), channel_id=1, source_target_pairs={{0,1},{1,0},{2,3},{3,2},{4,5},{5,4},{6,7},{7,6},{8,9},{9,8},{10,11... | collective-permute-start | bytes 3080 | tf_op jit(solution)/shard_map/ppermute | solution.py:36
  381.1 4.2 collective-permute-start.18
  383.0 5.4 %collective-permute-start.16 = (bf16[128,4]{0,1:T(4,128)(2,1)S(1)}, bf16[128,4]{0,1:T(4,128)(2,1)S(1)}, u32[]{:S(2)}, u32[]{:S(2)}) collective-permute-start(bf16[128,4]{0,1:T(4,128)(2,1)S(1)} %fusion.83), channel_id=1, source_target_pairs={{0,2},{2,0},{1,3},{3,1},{4,6},{6,4},{5,7},{7,5},{8,10},{10,8},{9,1... | collective-permute-start | bytes 3080 | tf_op jit(solution)/shard_map/ppermute | solution.py:36
  385.3 4.3 %collective-permute-start.19 = (bf16[128,4]{0,1:T(4,128)(2,1)S(1)}, bf16[128,4]{0,1:T(4,128)(2,1)S(1)}, u32[]{:S(2)}, u32[]{:S(2)}) collective-permute-start(bf16[128,4]{0,1:T(4,128)(2,1)S(1)} %get-tuple-element.8), channel_id=1, source_target_pairs={{0,2},{2,0},{1,3},{3,1},{4,6},{6,4},{5,7},{7,5},{8,10},{10,8},{9,1... | collective-permute-start | bytes 3080 | tf_op jit(solution)/shard_map/ppermute | solution.py:36
  391.3 4.8 %collective-permute-start.15 = (bf16[128,4,128]{2,0,1:T(8,128)(2,1)S(1)}, bf16[128,4,128]{2,0,1:T(8,128)(2,1)S(1)}, u32[]{:S(2)}, u32[]{:S(2)}) collective-permute-start(bf16[128,4,128]{2,0,1:T(8,128)(2,1)S(1)} %get-tuple-element.51), channel_id=1, source_target_pairs={{0,1},{1,0},{2,3},{3,2},{4,5},{5,4},{6,7},{7,6},{8,9},{9,8},{10,11... | collective-permute-start | bytes 393224 | tf_op jit(solution)/shard_map/ppermute | solution.py:36
  396.4 6.6 %collective-permute-start.17 = (bf16[128,4,128]{2,0,1:T(8,128)(2,1)S(1)}, bf16[128,4,128]{2,0,1:T(8,128)(2,1)S(1)}, u32[]{:S(2)}, u32[]{:S(2)}) collective-permute-start(bf16[128,4,128]{2,0,1:T(8,128)(2,1)S(1)} %get-tuple-element.12), channel_id=1, source_target_pairs={{0,2},{2,0},{1,3},{3,1},{4,6},{6,4},{5,7},{7,5},{8,10},{10,8},{9,1... | collective-permute-start | bytes 393224 | tf_op jit(solution)/shard_map/ppermute | solution.py:36
Sparse Core Ops, SparseCore 0:
  166.9 64.7 all-gather.2
  286.6 66.0 all-gather.4
